TPU v7x, 32 devices: a whole 2x2x4 slice. The times are simulated.
32 devices in a mesh: ep: 16 (over z, y, x), tp: 2 (over core).
Axes of the slice: x: 2, y: 2, z: 4, core: 2. Of those that a mesh axis runs over, the one named last changes fastest.
Arguments:
- stream: bfloat16 [1024, 2048], P('ep', 'tp'), may hold values from -40 to 40
- conv_state: bfloat16 [1024, 3, 2048], P('ep', None, 'tp'), may hold values from -5 to 5
- recur_state: float32 [1024, 2048], P('ep', 'tp'), may hold values from -5 to 5
- mix_gain: float32 [2048], replicated, may hold values from 0.1 to 1.9
- branch_weight: bfloat16 [2048, 2048], P(None, 'tp'), may hold values from -0.125 to 0.125
- gate_weight: bfloat16 [2048, 2048], P(None, 'tp'), may hold values from -0.125 to 0.125
- conv_taps: float32 [4, 2048], P(None, 'tp'), may hold values from -3 to 3
- recur_map: bfloat16 [16, 128, 128], P('tp'), may hold values from -0.5 to 0.5
- input_map: bfloat16 [16, 128, 128], P('tp'), may hold values from -0.5 to 0.5
- decay_logit: float32 [2048], P('tp'), may hold values from -1 to 6
- out_weight: bfloat16 [2048, 2048], P(None, 'tp'), may hold values from -0.125 to 0.125
- moe_gain: float32 [2048], replicated, may hold values from 0.1 to 1.9
- route_ids: int32 [1024, 6], P('ep'), may hold values from 0 to 15, all different within a row; in each aligned block of 64 rows (0 to 63, 64 to 127, ...) at most 64 rows name the same one
- route_weights: float32 [1024, 6], P('ep'), may hold values from 0.2 to 1
- expert_gate: bfloat16 [16, 2048, 512], P('ep', None, 'tp'), may hold values from -0.125 to 0.125
- expert_up: bfloat16 [16, 2048, 512], P('ep', None, 'tp'), may hold values from -0.125 to 0.125
- expert_down: bfloat16 [16, 512, 2048], P('ep', None, 'tp'), may hold values from -0.25 to 0.25
- dense_gate: bfloat16 [2048, 512], P(None, 'tp'), may hold values from -0.125 to 0.125
- dense_up: bfloat16 [2048, 512], P(None, 'tp'), may hold values from -0.125 to 0.125
- dense_down: bfloat16 [512, 2048], P(None, 'tp'), may hold values from -0.25 to 0.25
- dense_scale: float32 [2048], P('tp'), may hold values from 0.1 to 1.9
Outputs:
- result: bfloat16 [1024, 2048], P('ep', 'tp')
- new_state: float32 [1024, 2048], P('ep', 'tp')
- new_conv: bfloat16 [1024, 3, 2048], P('ep', None, 'tp')
Inputs may be any that keep to these rules, and one draw needn't show every extreme that they name: `route_ids`: each row names 6 different experts; among the rows of one index of ep no expert is named by more than 64 rows, and in every draw some expert is named by exactly 64 rows of some index.
All inputs are finite; a program needn't handle non-finite values.
Results may differ from a plain program's by a relative error of at most 0.014.
Values may be sent and summed in bfloat16 or wider, within the bound.
A program may use at most 128 MiB of HBM per device.

v0:
```python
import functools

import jax
import jax.numpy as jnp
from jax import lax
from jax.experimental import pallas as pl
from jax.experimental.pallas import tpu as pltpu
from jax.sharding import PartitionSpec as P

BF16 = jnp.bfloat16
F32 = jnp.float32
VMEM = pl.BlockSpec(memory_space=pltpu.VMEM)
ANY = pl.BlockSpec(memory_space=pl.ANY)


def dot(a, b):
    return jnp.dot(a, b, preferred_element_type=F32)


def remote(src, dst, send_sem, recv_sem, device):
    return pltpu.make_async_remote_copy(
        src_ref=src,
        dst_ref=dst,
        send_sem=send_sem,
        recv_sem=recv_sem,
        device_id=device,
        device_id_type=pl.DeviceIdType.MESH,
    )


def row_sums(rows):
    return (
        jnp.sum(rows, axis=1, keepdims=True),
        jnp.sum(rows * rows, axis=1, keepdims=True),
    )


def neg_expm1(y):
    series = 1.0 + y / 8.0
    for order in range(7, 1, -1):
        series = 1.0 + y / order * series
    return jnp.where(y > -0.3, -y * series, 1.0 - jnp.exp(y))


def norm_pair(own, own_sums, peer, gain_ref, t, out_ref):
    width = own.shape[1]
    peer_sums = row_sums(peer)
    mean = (own_sums[0] + peer_sums[0]) / (2 * width)
    var = (own_sums[1] + peer_sums[1]) / (2 * width) - mean * mean
    scale = lax.rsqrt(var + 1e-05)
    for slot, (rows, half) in enumerate(((own, t), (peer, 1 - t))):
        out_ref[slot] = ((rows - mean) * scale * gain_ref[half]).astype(BF16)


def mixer_kernel(
    stream_ref,
    part_ref,
    state_ref,
    gain_ref,
    branch_hbm,
    gate_hbm,
    taps_ref,
    rmap_ref,
    imap_ref,
    decay_ref,
    out_hbm,
    gain2_ref,
    branch_ref,
    new_state_ref,
    resid_ref,
    n2_ref,
    branch_w,
    gate_w,
    out_w,
    peer_ref,
    nrm_ref,
    mix_ref,
    res_ref,
    load_sem,
    send_sem,
    recv_sem,
):
    t = lax.axis_index("tp")
    partner = {"tp": 1 - t}
    loads = [
        pltpu.make_async_copy(src, dst, load_sem.at[i])
        for i, (src, dst) in enumerate(
            ((branch_hbm, branch_w), (gate_hbm, gate_w), (out_hbm, out_w))
        )
    ]
    for load in loads:
        load.start()
    barrier = pltpu.get_barrier_semaphore()
    pl.semaphore_signal(barrier, inc=1, device_id=partner, device_id_type=pl.DeviceIdType.MESH)
    pl.semaphore_wait(barrier, 1)
    first = remote(stream_ref, peer_ref, send_sem.at[0], recv_sem.at[0], partner)
    first.start()
    own = stream_ref[...].astype(F32)
    own_sums = row_sums(own)
    first.wait_recv()
    norm_pair(own, own_sums, peer_ref[...].astype(F32), gain_ref, t, nrm_ref)

    width = stream_ref.shape[1]
    block = rmap_ref.shape[1]
    chunk = 2 * block
    loads[0].wait()
    loads[1].wait()
    for c in range(width // chunk):
        cols = pl.ds(c * chunk, chunk)
        branch = dot(nrm_ref[0], branch_w[t, :, cols]) + dot(nrm_ref[1], branch_w[1 - t, :, cols])
        branch = branch.astype(BF16)
        branch_ref[:, cols] = branch
        gate = dot(nrm_ref[0], gate_w[t, :, cols]) + dot(nrm_ref[1], gate_w[1 - t, :, cols])
        gate = gate.astype(BF16).astype(F32)
        conv = (branch.astype(F32) * taps_ref[3:4, cols] + part_ref[:, cols]).astype(BF16)
        rec, inp = [], []
        for b in range(2):
            piece = conv[:, b * block : (b + 1) * block]
            rec.append(dot(piece, rmap_ref[2 * c + b]))
            inp.append(dot(piece, imap_ref[2 * c + b]))
        recur_gate = jax.nn.sigmoid(jnp.concatenate(rec, axis=1))
        input_gate = jax.nn.sigmoid(jnp.concatenate(inp, axis=1))
        logit = -decay_ref[:, cols]
        softplus = jnp.maximum(logit, 0.0) + jnp.log1p(jnp.exp(-jnp.abs(logit)))
        log_decay = -8.0 * recur_gate * softplus
        driven = jnp.sqrt(neg_expm1(2.0 * log_decay)) * (input_gate * conv.astype(F32))
        state = jnp.exp(log_decay) * state_ref[:, cols] + driven
        new_state_ref[:, cols] = state
        gelu = 0.5 * gate * (1.0 + jnp.tanh(0.7978845608028654 * (gate + 0.044715 * gate**3)))
        mix_ref[0, :, cols] = (gelu * state).astype(BF16)
    second = remote(mix_ref.at[0], mix_ref.at[1], send_sem.at[1], recv_sem.at[1], partner)
    second.start()
    loads[2].wait()
    mixed = dot(mix_ref[0], out_w[t])
    second.wait_recv()
    mixed = (mixed + dot(mix_ref[1], out_w[1 - t])).astype(BF16)
    resid = (own + mixed.astype(F32)).astype(BF16)
    res_ref[0] = resid
    third = remote(res_ref.at[0], res_ref.at[1], send_sem.at[2], recv_sem.at[2], partner)
    third.start()
    resid_ref[...] = resid
    resid = resid.astype(F32)
    sums = row_sums(resid)
    third.wait_recv()
    norm_pair(resid, sums, res_ref[1].astype(F32), gain2_ref, t, n2_ref)
    for copy in (first, second, third):
        copy.wait_send()


def flipped(q, r):
    return (q // 2 + r // 2) % 2 * 2 + (q + r) % 2


def layer_kernel(
    peers,
    stream_hbm,
    conv_hbm,
    state_hbm,
    gain_hbm,
    branch_hbm,
    gate_hbm,
    taps_hbm,
    rmap_hbm,
    imap_hbm,
    decay_hbm,
    out_hbm,
    gain2_hbm,
    ids_hbm,
    weights_hbm,
    scale_hbm,
    eg_hbm,
    eu_hbm,
    ed_hbm,
    dg_hbm,
    du_hbm,
    dd_hbm,
    result_ref,
    new_state_ref,
    new_conv_ref,
    stream_ref,
    conv_ref,
    state_ref,
    gain_ref,
    branch_w,
    gate_w,
    taps_ref,
    rmap_ref,
    imap_ref,
    decay_ref,
    out_w,
    gain2_ref,
    ids_ref,
    weights_ref,
    scale_ref,
    eg,
    eu,
    ed,
    dg,
    du,
    dd,
    peer_ref,
    nrm_ref,
    mix_ref,
    res_ref,
    inc,
    hid,
    dhid,
    snd,
    zbuf,
    got_d,
    got_x,
    got_y,
    got_z,
    base_ref,
    wsend,
    wrecv,
    load_sem,
    m_send,
    m_recv,
    w_send,
    w_recv,
    p_send,
    p_recv,
    h_send,
    h_recv,
    link_send,
    link_recv,
    back_send,
    back_recv,
):
    e = lax.axis_index("ep")
    t = lax.axis_index("tp")
    partner = {"tp": 1 - t}
    depth = peers // 4
    z = e // 4
    q = e % 4
    x_near = {"ep": 4 * z + flipped(q, 1)}
    y_near = {"ep": 4 * z + flipped(q, 2)}
    rows, width = stream_ref.shape
    pairs = (
        (stream_hbm, stream_ref),
        (gain_hbm, gain_ref),
        (branch_hbm, branch_w),
        (gate_hbm, gate_w),
        (conv_hbm, conv_ref),
        (taps_hbm, taps_ref),
        (rmap_hbm, rmap_ref),
        (imap_hbm, imap_ref),
        (decay_hbm, decay_ref),
        (state_hbm, state_ref),
        (out_hbm, out_w),
        (gain2_hbm, gain2_ref),
        (ids_hbm, ids_ref),
        (weights_hbm, weights_ref),
        (scale_hbm, scale_ref),
        (dg_hbm, dg),
        (du_hbm, du),
        (dd_hbm, dd),
        (eg_hbm, eg),
        (eu_hbm, eu),
        (ed_hbm, ed),
    )
    loads = [pltpu.make_async_copy(a, b, load_sem.at[i]) for i, (a, b) in enumerate(pairs)]
    for i in (0, 1, 12, 13, 2, 3, 4, 5, 6, 7, 8, 9):
        loads[i].start()
    barrier = pltpu.get_barrier_semaphore()
    pl.semaphore_signal(barrier, inc=1, device_id=partner, device_id_type=pl.DeviceIdType.MESH)

    @pl.loop(1, peers)
    def _(offset):
        pl.semaphore_signal(
            barrier,
            inc=1,
            device_id={"ep": lax.rem(e + offset, peers)},
            device_id_type=pl.DeviceIdType.MESH,
        )

    loads[0].wait()
    pl.semaphore_wait(barrier, peers)
    first = remote(stream_ref, peer_ref, m_send.at[0], m_recv.at[0], partner)
    first.start()
    own = stream_ref[...].astype(F32)
    own_sums = row_sums(own)

    loads[12].wait()
    loads[13].wait()
    ids = ids_ref[...]
    weights = weights_ref[...]
    lanes = wsend.shape[2]
    for d in range(peers):
        row = jnp.sum(jnp.where(ids == d, weights, 0.0), axis=0, keepdims=True)
        wsend[d] = jnp.concatenate([row, jnp.zeros((1, lanes - rows), F32)], axis=1)

    def weighing(r, o):
        there = (z + o) % depth
        d = 4 * there + flipped(q, r)
        slot = 4 * z + r
        return remote(wsend.at[d], wrecv.at[slot], w_send.at[d], w_recv.at[slot], {"ep": d})

    places = [(r, o) for r in range(4) for o in range(depth) if r or o]
    for r, o in places:
        weighing(r, o).start()

    loads[1].wait()
    first.wait_recv()
    norm_pair(own, own_sums, peer_ref[...].astype(F32), gain_ref, t, nrm_ref)
    for load in loads[2:10]:
        load.wait()
    for i in (10, 11, 14, 15, 16, 17, 18, 19, 20):
        loads[i].start()
    block = rmap_ref.shape[1]
    chunk = 2 * block
    for c in range(width // chunk):
        cols = pl.ds(c * chunk, chunk)
        branch = dot(nrm_ref[0], branch_w[t, :, cols]) + dot(nrm_ref[1], branch_w[1 - t, :, cols])
        branch = branch.astype(BF16)
        gate = dot(nrm_ref[0], gate_w[t, :, cols]) + dot(nrm_ref[1], gate_w[1 - t, :, cols])
        gate = gate.astype(BF16).astype(F32)
        conv = branch.astype(F32) * taps_ref[3:4, cols]
        for i in range(3):
            conv = conv + conv_ref[i, :, cols].astype(F32) * taps_ref[i : i + 1, cols]
        conv = conv.astype(BF16)
        new_conv_ref[0, :, cols] = conv_ref[1, :, cols]
        new_conv_ref[1, :, cols] = conv_ref[2, :, cols]
        new_conv_ref[2, :, cols] = branch
        rec, inp = [], []
        for b in range(2):
            piece = conv[:, b * block : (b + 1) * block]
            rec.append(dot(piece, rmap_ref[2 * c + b]))
            inp.append(dot(piece, imap_ref[2 * c + b]))
        recur_gate = jax.nn.sigmoid(jnp.concatenate(rec, axis=1))
        input_gate = jax.nn.sigmoid(jnp.concatenate(inp, axis=1))
        logit = -decay_ref[:, cols]
        softplus = jnp.maximum(logit, 0.0) + jnp.log1p(jnp.exp(-jnp.abs(logit)))
        log_decay = -8.0 * recur_gate * softplus
        driven = jnp.sqrt(neg_expm1(2.0 * log_decay)) * (input_gate * conv.astype(F32))
        state = jnp.exp(log_decay) * state_ref[:, cols] + driven
        new_state_ref[:, cols] = state
        gelu = 0.5 * gate * (1.0 + jnp.tanh(0.7978845608028654 * (gate + 0.044715 * gate**3)))
        mix_ref[0, :, cols] = (gelu * state).astype(BF16)
    second = remote(mix_ref.at[0], mix_ref.at[1], m_send.at[1], m_recv.at[1], partner)
    second.start()
    loads[10].wait()
    mixed = dot(mix_ref[0], out_w[t])
    second.wait_recv()
    mixed = (mixed + dot(mix_ref[1], out_w[1 - t])).astype(BF16)
    resid = (own + mixed.astype(F32)).astype(BF16)
    res_ref[0] = resid
    third = remote(res_ref.at[0], res_ref.at[1], m_send.at[2], m_recv.at[2], partner)
    third.start()
    resid = resid.astype(F32)
    sums = row_sums(resid)
    loads[11].wait()
    third.wait_recv()
    norm_pair(resid, sums, res_ref[1].astype(F32), gain2_ref, t, nrm_ref)
    inc[0, 4 * z] = nrm_ref[0]
    inc[1, 4 * z] = nrm_ref[1]

    split = width // 2

    def at(o):
        return (z + depth - o) % depth

    def z_copy(o):
        there = {"ep": 4 * ((z + o) % depth) + q}
        return remote(
            inc.at[0, 4 * z], inc.at[0, 4 * z], link_send.at[0, o], link_recv.at[0, z], there
        )

    def z_wait(o):
        j = at(o)
        mine = inc.at[0, 4 * j]
        remote(mine, mine, link_send.at[0, o], link_recv.at[0, j], partner).wait_recv()

    def side_copy(r, o):
        j = at(o)
        return remote(
            inc.at[0, 4 * j],
            inc.at[0, 4 * j + r],
            link_send.at[r, j],
            link_recv.at[r, j],
            x_near if r == 1 else y_near,
        )

    def d_copy(r, o):
        j = at(o)
        cols = pl.ds((r - 1) * split, split)
        return remote(
            inc.at[0, 4 * j + 3 - r, :, cols],
            inc.at[0, 4 * j + 3, :, cols],
            link_send.at[2 + r, j],
            link_recv.at[2 + r, j],
            x_near if r == 1 else y_near,
        )

    def p_copy(r, o):
        slot = 4 * at(o) + r
        return remote(inc.at[0, slot], inc.at[1, slot], p_send.at[slot], p_recv.at[slot], partner)

    for o in range(1, depth):
        z_copy(o).start()
    side_copy(1, 0).start()
    side_copy(2, 0).start()

    for load in loads[14:18]:
        load.wait()
    dense_gate = dot(nrm_ref[0], dg[t]) + dot(nrm_ref[1], dg[1 - t])
    dense_up = dot(nrm_ref[0], du[t]) + dot(nrm_ref[1], du[1 - t])
    dhid[0] = (jax.nn.silu(dense_gate) * dense_up).astype(BF16)
    dense_copy = remote(dhid.at[0], dhid.at[1], m_send.at[3], m_recv.at[3], partner)
    dense_copy.start()

    def along(o):
        z_wait(o)
        side_copy(1, o).start()
        side_copy(2, o).start()
        p_copy(0, o).start()

    def near(o):
        side_copy(1, o).wait_recv()
        d_copy(2, o).start()
        p_copy(1, o).start()
        side_copy(2, o).wait_recv()
        d_copy(1, o).start()
        p_copy(2, o).start()

    def h_copy(o):
        part = pl.ds(4 * at(o), 4)
        return remote(hid.at[0, part], hid.at[1, part], h_send.at[o], h_recv.at[o], partner)

    def upward(o):
        for r in range(4):
            if r or o:
                p_copy(r, o).wait_recv()
        part = pl.ds(4 * at(o), 4)
        mine = inc[0, part].reshape(4 * rows, width)
        peer = inc[1, part].reshape(4 * rows, width)
        gate = dot(mine, eg[t]) + dot(peer, eg[1 - t])
        up = dot(mine, eu[t]) + dot(peer, eu[1 - t])
        hid[0, part] = (jax.nn.silu(gate) * up).astype(BF16).reshape(4, rows, -1)
        h_copy(o).start()

    spread = lax.broadcasted_iota(jnp.int32, (rows, lanes), 0) == lax.broadcasted_iota(
        jnp.int32, (rows, lanes), 1
    )

    def downward(o):
        base_slot = 4 * at(o)
        part = pl.ds(base_slot, 4)
        cols = []
        for r in range(4):
            row = wrecv[base_slot + r]
            cols.append(jnp.sum(jnp.where(spread, row, 0.0), axis=1, keepdims=True))
        h_copy(o).wait_recv()
        mine = hid[0, part].reshape(4 * rows, -1)
        peer = hid[1, part].reshape(4 * rows, -1)
        served = dot(mine, ed[t]) + dot(peer, ed[1 - t])
        served = served * jnp.concatenate(cols, axis=0)
        snd[part] = served.astype(BF16).reshape(4, rows, width)
        bd_copy(1, o).start()
        bd_copy(2, o).start()

    def bd_copy(r, o):
        j = at(o)
        cols = pl.ds((r - 1) * split, split)
        return remote(
            snd.at[4 * j + 3, :, cols],
            got_d.at[j, :, cols],
            back_send.at[2 + r, j],
            back_recv.at[2 + r, j],
            x_near if r == 1 else y_near,
        )

    def side_back(r, o):
        j = at(o)
        return remote(
            snd.at[4 * j + r],
            (got_x if r == 1 else got_y).at[j],
            back_send.at[r, j],
            back_recv.at[r, j],
            x_near if r == 1 else y_near,
        )

    def bz_copy(o):
        j = at(o)
        there = {"ep": 4 * j + q}
        return remote(zbuf.at[j], got_z.at[z], back_send.at[0, j], back_recv.at[0, z], there)

    def bz_wait(o):
        j = at(o)
        remote(zbuf.at[j], got_z.at[j], back_send.at[0, j], back_recv.at[0, j], partner).wait_recv()

    def joined(o):
        j = at(o)
        for r in (1, 2):
            bd_copy(r, o).wait_recv()
            cols = pl.ds((r - 1) * split, split)
            slot = 4 * j + 3 - r
            both = snd[slot, :, cols].astype(F32) + got_d[j, :, cols].astype(F32)
            snd[slot, :, cols] = both.astype(BF16)
            side_back(3 - r, o).start()

    def summed(o):
        j = at(o)
        side_back(1, o).wait_recv()
        side_back(2, o).wait_recv()
        total = snd[4 * j].astype(F32) + got_x[j].astype(F32) + got_y[j].astype(F32)
        if o:
            zbuf[j] = total.astype(BF16)
            bz_copy(o).start()
        return total

    along(1)
    near(0)
    for r, o in places:
        slot = 4 * at(o) + r
        remote(wsend.at[0], wrecv.at[slot], w_send.at[0], w_recv.at[slot], partner).wait_recv()
    mine = jnp.sum(jnp.where(ids == e, weights, 0.0), axis=0, keepdims=True)
    wrecv[4 * z] = jnp.concatenate([mine, jnp.zeros((1, lanes - rows), F32)], axis=1)
    dense = dot(dhid[0], dd[t])
    dense_copy.wait_recv()
    dense = (dense + dot(dhid[1], dd[1 - t])).astype(BF16)
    base_ref[...] = resid + scale_ref[...] * dense.astype(F32)
    for load in loads[18:]:
        load.wait()

    for step in range(1, depth + 3):
        if step + 1 < depth:
            along(step + 1)
        if step < depth:
            near(step)
        if step <= depth:
            d_copy(1, step - 1).wait_recv()
            d_copy(2, step - 1).wait_recv()
            p_copy(3, step - 1).start()
        if 2 <= step <= depth + 1:
            joined(step - 2)
        if step <= depth:
            upward(step - 1)
            downward(step - 1)
        if 3 <= step:
            part_sum = summed(step - 3)
            if step == 3:
                base_ref[...] += part_sum
    total = base_ref[...]
    for o in range(1, depth):
        bz_wait(o)
        total = total + got_z[at(o)].astype(F32)
    result_ref[...] = total.astype(BF16)

    for copy in (first, second, third, dense_copy):
        copy.wait_send()
    for r, o in places:
        weighing(r, o).wait_send()
        p_copy(r, o).wait_send()
    for o in range(depth):
        h_copy(o).wait_send()
        if o:
            z_copy(o).wait_send()
            bz_copy(o).wait_send()
        for r in (1, 2):
            for copy in (side_copy, d_copy, side_back, bd_copy):
                copy(r, o).wait_send()


def expert_kernel(
    full,
    peers,
    group,
    n2_ref,
    out_ref,
    resid_ref,
    ids_ref,
    weights_ref,
    scale_ref,
    eg_hbm,
    eu_hbm,
    ed_hbm,
    dg_hbm,
    du_hbm,
    dd_hbm,
    *refs,
):
    if full:
        result_ref, *refs = refs
    else:
        dense_ref, back_ref, *refs = refs
    (
        eg,
        eu,
        ed,
        dg,
        du,
        dd,
        inc,
        hid,
        src,
        ret,
        dhid,
        load_sem,
        own_sem,
        x_send,
        x_recv,
        f_send,
        f_recv,
        h_send,
        h_recv,
        r_send,
        r_recv,
        d_sem,
    ) = refs
    e = lax.axis_index("ep")
    t = lax.axis_index("tp")
    partner = {"tp": 1 - t}
    groups = peers // group
    cap = inc.shape[2]
    width = inc.shape[3]
    loads = [
        pltpu.make_async_copy(a, b, load_sem.at[i])
        for i, (a, b) in enumerate(
            ((dg_hbm, dg), (du_hbm, du), (dd_hbm, dd), (eg_hbm, eg), (eu_hbm, eu), (ed_hbm, ed))
        )
    ]
    for load in loads:
        load.start()

    def outgoing(offset):
        return n2_ref.at[0] if full else out_ref.at[lax.rem(e + offset, peers)]

    keep = pltpu.make_async_copy(outgoing(0), inc.at[0, 0], own_sem)
    keep.start()
    barrier = pltpu.get_barrier_semaphore()
    pl.semaphore_signal(barrier, inc=1, device_id=partner, device_id_type=pl.DeviceIdType.MESH)

    @pl.loop(1, peers)
    def _(offset):
        pl.semaphore_signal(
            barrier,
            inc=1,
            device_id={"ep": lax.rem(e + offset, peers)},
            device_id_type=pl.DeviceIdType.MESH,
        )

    pl.semaphore_wait(barrier, peers)

    def sending(offset):
        return remote(
            outgoing(offset),
            inc.at[0, offset],
            x_send.at[offset],
            x_recv.at[offset],
            {"ep": lax.rem(e + offset, peers)},
        )

    @pl.loop(1, peers)
    def _(offset):
        sending(offset).start()

    for load in loads[:3]:
        load.wait()
    rows0, rows1 = n2_ref[0], n2_ref[1]
    dense_gate = dot(rows0, dg[t]) + dot(rows1, dg[1 - t])
    dense_up = dot(rows0, du[t]) + dot(rows1, du[1 - t])
    dhid[0] = (jax.nn.silu(dense_gate) * dense_up).astype(BF16)
    dense_copy = remote(dhid.at[0], dhid.at[1], d_sem.at[0], d_sem.at[1], partner)
    dense_copy.start()
    dense = dot(dhid[0], dd[t])
    dense_copy.wait()
    dense = (dense + dot(dhid[1], dd[1 - t])).astype(BF16)
    keep.wait()
    for load in loads[3:]:
        load.wait()

    def forwarding(g):
        part = pl.ds(g * group, group)
        return remote(inc.at[0, part], inc.at[1, part], f_send.at[g], f_recv.at[g], partner)

    def hiding(g):
        part = pl.ds(g * group, group)
        return remote(hid.at[0, part], hid.at[1, part], h_send.at[g], h_recv.at[g], partner)

    def returning(offset):
        return remote(
            src.at[offset],
            ret.at[offset],
            r_send.at[offset],
            r_recv.at[offset],
            {"ep": lax.rem(e + peers - offset, peers)},
        )

    def arrive(g):
        @pl.loop(max(1, g * group), (g + 1) * group)
        def _(offset):
            sending(offset).wait_recv()

        forwarding(g).start()

    def upward(g):
        forwarding(g).wait_recv()
        part = pl.ds(g * group, group)
        own = inc[0, part].reshape(group * cap, width)
        peer = inc[1, part].reshape(group * cap, width)
        gate = dot(own, eg[t]) + dot(peer, eg[1 - t])
        up = dot(own, eu[t]) + dot(peer, eu[1 - t])
        hidden = (jax.nn.silu(gate) * up).astype(BF16)
        hid[0, part] = hidden.reshape(group, cap, -1)
        hiding(g).start()

    def downward(g):
        hiding(g).wait_recv()
        part = pl.ds(g * group, group)
        own = hid[0, part].reshape(group * cap, -1)
        peer = hid[1, part].reshape(group * cap, -1)
        served = dot(own, ed[t]) + dot(peer, ed[1 - t])
        src[part] = served.astype(BF16).reshape(group, cap, width)

        @pl.loop(max(1, g * group), (g + 1) * group)
        def _(offset):
            returning(offset).start()

    for step in range(groups + 2):
        if step < groups:
            arrive(step)
        if 1 <= step <= groups:
            upward(step - 1)
        if step >= 2:
            downward(step - 2)

    if full:
        total = resid_ref[...].astype(F32) + scale_ref[...] * dense.astype(F32)
        ids = ids_ref[...]
        weights = weights_ref[...]

        def weight(offset):
            chosen = ids == lax.rem(e + offset, peers)
            return jnp.sum(jnp.where(chosen, weights, 0.0), axis=1, keepdims=True)

        routed = weight(0) * src[0].astype(F32)
        for offset in range(1, peers):
            returning(offset).wait_recv()
            routed = routed + weight(offset) * ret[offset].astype(F32)
        result_ref[...] = (total + routed).astype(BF16)
    else:
        dense_ref[...] = dense
        back_ref[0] = src[0]

        @pl.loop(1, peers)
        def _(offset):
            returning(offset).wait_recv()
            back_ref[offset] = ret[offset]

    @pl.loop(1, peers)
    def _(offset):
        sending(offset).wait_send()
        returning(offset).wait_send()

    @pl.loop(0, groups)
    def _(g):
        forwarding(g).wait_send()
        hiding(g).wait_send()


def halves(weight):
    return weight.reshape(2, weight.shape[0] // 2, weight.shape[1])


def per_device(
    stream,
    conv_state,
    recur_state,
    mix_gain,
    branch_weight,
    gate_weight,
    conv_taps,
    recur_map,
    input_map,
    decay_logit,
    out_weight,
    moe_gain,
    route_ids,
    route_weights,
    expert_gate,
    expert_up,
    expert_down,
    dense_gate,
    dense_up,
    dense_down,
    dense_scale,
):
    rows, width = stream.shape
    dma = pltpu.SemaphoreType.DMA
    top = route_ids.shape[1]
    peers = lax.axis_size("ep")
    cap = max(2, min(rows, 3 * rows * top // peers))
    if cap == rows and peers % 8 == 0:
        operands = (
            stream,
            conv_state.transpose(1, 0, 2),
            recur_state,
            mix_gain.reshape(2, 1, width),
            halves(branch_weight),
            halves(gate_weight),
            conv_taps,
            recur_map,
            input_map,
            decay_logit.reshape(1, width),
            halves(out_weight),
            moe_gain.reshape(2, 1, width),
            route_ids.T,
            route_weights.T,
            dense_scale.reshape(1, width),
            halves(expert_gate[0]),
            halves(expert_up[0]),
            halves(expert_down[0]),
            halves(dense_gate),
            halves(dense_up),
            halves(dense_down),
        )
        depth = peers // 4
        hidden = expert_gate.shape[2]
        lanes = -(-rows // 128) * 128
        column = pltpu.VMEM((depth, rows, width), BF16)
        result, new_state, new_conv = pl.pallas_call(
            functools.partial(layer_kernel, peers),
            out_shape=(
                jax.ShapeDtypeStruct((rows, width), BF16),
                jax.ShapeDtypeStruct((rows, width), F32),
                jax.ShapeDtypeStruct((3, rows, width), BF16),
            ),
            in_specs=[ANY] * len(operands),
            out_specs=[VMEM] * 3,
            scratch_shapes=[pltpu.VMEM(a.shape, a.dtype) for a in operands]
            + [pltpu.VMEM((rows, width), BF16)]
            + [pltpu.VMEM((2, rows, width), BF16)] * 3
            + [
                pltpu.VMEM((2, peers, rows, width), BF16),
                pltpu.VMEM((2, peers, rows, hidden), BF16),
                pltpu.VMEM((2, rows, dense_gate.shape[1]), BF16),
                pltpu.VMEM((peers, rows, width), BF16),
            ]
            + [column] * 5
            + [pltpu.VMEM((rows, width), F32)]
            + [pltpu.VMEM((peers, 1, lanes), F32)] * 2
            + [dma((len(operands),))]
            + [dma((4,))] * 2
            + [dma((peers,))] * 4
            + [dma((depth,))] * 2
            + [dma((5, depth))] * 4,
            compiler_params=pltpu.CompilerParams(
                collective_id=2, has_side_effects=True, vmem_limit_bytes=63 * 1024 * 1024
            ),
            name="layer",
        )(*operands)
        return result, new_state, new_conv.transpose(1, 0, 2)
    conv_part = sum(conv_state[:, i].astype(F32) * conv_taps[i] for i in range(3))
    branch_in, new_state, resid, n2 = pl.pallas_call(
        mixer_kernel,
        out_shape=(
            jax.ShapeDtypeStruct((rows, width), BF16),
            jax.ShapeDtypeStruct((rows, width), F32),
            jax.ShapeDtypeStruct((rows, width), BF16),
            jax.ShapeDtypeStruct((2, rows, width), BF16),
        ),
        in_specs=[VMEM] * 4 + [ANY] * 2 + [VMEM] * 4 + [ANY, VMEM],
        out_specs=[VMEM] * 4,
        scratch_shapes=[pltpu.VMEM((2, width, width), BF16)] * 3
        + [pltpu.VMEM((rows, width), BF16)]
        + [pltpu.VMEM((2, rows, width), BF16)] * 3
        + [dma((3,))] * 3,
        compiler_params=pltpu.CompilerParams(
            collective_id=0, has_side_effects=True, vmem_limit_bytes=48 * 1024 * 1024
        ),
        name="mixer",
    )(
        stream,
        conv_part,
        recur_state,
        mix_gain.reshape(2, 1, width),
        halves(branch_weight),
        halves(gate_weight),
        conv_taps,
        recur_map,
        input_map,
        decay_logit.reshape(1, width),
        halves(out_weight),
        moe_gain.reshape(2, 1, width),
    )
    new_conv = jnp.concatenate([conv_state[:, 1:], branch_in[:, None]], axis=1)

    full = cap == rows
    if full:
        outgoing = jnp.zeros((8, 128), BF16)
    else:
        cap = -(-cap // 16) * 16
        flat_ids = route_ids.reshape(-1)
        one_hot = (flat_ids[:, None] == jnp.arange(peers, dtype=jnp.int32)[None, :]).astype(jnp.int32)
        rank = jnp.sum(one_hot * (jnp.cumsum(one_hot, axis=0) - 1), axis=1)
        slots = (flat_ids * cap + rank).reshape(rows, top)
        table = jnp.sum(
            (slots[:, :, None] == jnp.arange(peers * cap, dtype=jnp.int32)).astype(BF16), axis=1
        )
        outgoing = lax.dot_general(
            table, n2[0], (((0,), (0,)), ((), ())), preferred_element_type=F32
        )
        outgoing = outgoing.astype(BF16).reshape(peers, cap, width)
    group = max(1, min(peers, 256 // cap))
    while peers % group:
        group -= 1
    groups = peers // group
    hidden = expert_gate.shape[2]
    out_shape = [jax.ShapeDtypeStruct((rows, width), BF16)]
    if not full:
        out_shape.append(jax.ShapeDtypeStruct((peers, cap, width), BF16))
    outs = pl.pallas_call(
        functools.partial(expert_kernel, full, peers, group),
        out_shape=out_shape,
        in_specs=[VMEM] * 6 + [ANY] * 6,
        out_specs=[VMEM] * len(out_shape),
        scratch_shapes=[
            pltpu.VMEM((2, width, hidden), BF16),
            pltpu.VMEM((2, width, hidden), BF16),
            pltpu.VMEM((2, hidden, width), BF16),
            pltpu.VMEM((2, width, dense_gate.shape[1]), BF16),
            pltpu.VMEM((2, width, dense_gate.shape[1]), BF16),
            pltpu.VMEM((2, dense_gate.shape[1], width), BF16),
            pltpu.VMEM((2, peers, cap, width), BF16),
            pltpu.VMEM((2, peers, cap, hidden), BF16),
            pltpu.VMEM((peers, cap, width), BF16),
            pltpu.VMEM((peers, cap, width), BF16),
            pltpu.VMEM((2, rows, dense_gate.shape[1]), BF16),
            dma((6,)),
            dma,
            dma((peers,)),
            dma((peers,)),
            dma((groups,)),
            dma((groups,)),
            dma((groups,)),
            dma((groups,)),
            dma((peers,)),
            dma((peers,)),
            dma((2,)),
        ],
        compiler_params=pltpu.CompilerParams(
            collective_id=1, has_side_effects=True, vmem_limit_bytes=56 * 1024 * 1024
        ),
        name="experts",
    )(
        n2,
        outgoing,
        resid,
        route_ids,
        route_weights,
        dense_scale.reshape(1, width),
        halves(expert_gate[0]),
        halves(expert_up[0]),
        halves(expert_down[0]),
        halves(dense_gate),
        halves(dense_up),
        halves(dense_down),
    )
    if full:
        return outs[0], new_state, new_conv
    dense_out, back = outs
    shifted = lax.rem(flat_ids - lax.axis_index("ep") + peers, peers)
    picked = back.reshape(peers * cap, width)[(shifted * cap + rank).reshape(rows, top)]
    routed = jnp.sum(picked.astype(F32) * route_weights[:, :, None], axis=1)
    result = (resid.astype(F32) + routed + dense_scale * dense_out.astype(F32)).astype(BF16)
    return result, new_state, new_conv


def solution(mesh):
    in_specs = (
        P("ep", "tp"),
        P("ep", None, "tp"),
        P("ep", "tp"),
        P(),
        P(None, "tp"),
        P(None, "tp"),
        P(None, "tp"),
        P("tp", None, None),
        P("tp", None, None),
        P("tp"),
        P(None, "tp"),
        P(),
        P("ep", None),
        P("ep", None),
        P("ep", None, "tp"),
        P("ep", None, "tp"),
        P("ep", None, "tp"),
        P(None, "tp"),
        P(None, "tp"),
        P(None, "tp"),
        P("tp"),
    )
    out_specs = (P("ep", "tp"), P("ep", "tp"), P("ep", None, "tp"))
    return jax.shard_map(
        per_device, mesh=mesh, in_specs=in_specs, out_specs=out_specs, check_vma=False
    )
```

profile of v0, /device:TPU:0, one launch (start us, length us, event | category | flops | bytes accessed | tf_op | source)
XLA Modules:
  0.0 72.6 jit_solution(6381917464000779354)
XLA Ops:
  0.6 66.9 %layer.1 = (bf16[64,1024]{1,0:T(8,128)(2,1)}, f32[64,1024]{1,0:T(8,128)}, bf16[3,64,1024]{2,1,0:T(8,128)(2,1)}) custom-call(bf16[64,1024]{1,0:T(8,128)(2,1)} %stream_hbm.1, bf16[3,64,1024]{2,1,0:T(8,128)(2,1)} %bitcast.27, f32[64,1024]{1,0:T(8,128)} %state_hbm.1, f32[2,1,1024]{2,1,0:T(1,128)} %bitcast.28, bf16[2,1024,1024]{2,1,0:T(8,128)(2,1)} %bitcast.17, ...), custom_call_target="tpu_custom_call" | custom-call | tf_op jit(solution)/shard_map/layer/pallas_call | solution.py:823
  67.6 1.6 %copy.27 = bf16[64,1024]{1,0:T(8,128)(2,1)} copy(bf16[64,1024]{1,0:T(8,128)(2,1)} %get-tuple-element.12) | data formatting | bytes 262144
  69.1 1.7 %copy.28 = f32[64,1024]{1,0:T(8,128)} copy(f32[64,1024]{1,0:T(8,128)} %get-tuple-element.13) | data formatting | bytes 524288
  70.8 1.8 %copy.29 = bf16[64,3,1024]{2,0,1:T(8,128)(2,1)} copy(bf16[64,3,1024]{2,0,1:T(8,128)(2,1)} %bitcast.26) | data formatting | bytes 786432
where the time goes:
time: 72.8 us; the launch traced here: 72.6 us
  Pallas kernels  66.9 us (92%)
  local copies, waits for them, and re-layouts  5 us (7%)
    pallas_call x1, Pallas kernels, per_device(): pl.pallas_call(functools.partial(layer_kernel, peers), out_shape=(jax.Sha...  66.9 us
    unnamed x3, local copies, waits for them, and re-layouts  5 us

commit v1 on v0

--- a/solution.py
+++ b/solution.py
@@ -11,6 +11,7 @@
 F32 = jnp.float32
 VMEM = pl.BlockSpec(memory_space=pltpu.VMEM)
 ANY = pl.BlockSpec(memory_space=pl.ANY)
+HBM = pl.BlockSpec(memory_space=pltpu.HBM)
 
 
 def dot(a, b):
@@ -760,6 +761,19 @@
         hiding(g).wait_send()
 
 
+def emit_kernel(a_in, b_in, c_in, a_out, b_out, c_out, a, b, c, sem):
+    sets = tuple(enumerate(((a_in, a, a_out), (b_in, b, b_out), (c_in, c, c_out))))
+    reads = [pltpu.make_async_copy(src, mid, sem.at[0, i]) for i, (src, mid, _) in sets]
+    writes = [pltpu.make_async_copy(mid, dst, sem.at[1, i]) for i, (_, mid, dst) in sets]
+    for read in reads:
+        read.start()
+    for read, write in zip(reads, writes):
+        read.wait()
+        write.start()
+    for write in writes:
+        write.wait()
+
+
 def halves(weight):
     return weight.reshape(2, weight.shape[0] // 2, weight.shape[1])
 
@@ -827,7 +841,7 @@
                 jax.ShapeDtypeStruct((rows, width), F32),
                 jax.ShapeDtypeStruct((3, rows, width), BF16),
             ),
-            in_specs=[ANY] * len(operands),
+            in_specs=[HBM] * len(operands),
             out_specs=[VMEM] * 3,
             scratch_shapes=[pltpu.VMEM(a.shape, a.dtype) for a in operands]
             + [pltpu.VMEM((rows, width), BF16)]
@@ -851,6 +865,16 @@
             ),
             name="layer",
         )(*operands)
+        result, new_state, new_conv = pl.pallas_call(
+            emit_kernel,
+            out_shape=tuple(jax.ShapeDtypeStruct(a.shape, a.dtype) for a in (result, new_state, new_conv)),
+            in_specs=[ANY] * 3,
+            out_specs=[ANY] * 3,
+            scratch_shapes=[pltpu.VMEM(a.shape, a.dtype) for a in (result, new_state, new_conv)]
+            + [dma((2, 3))],
+            compiler_params=pltpu.CompilerParams(vmem_limit_bytes=63 * 1024 * 1024),
+            name="emit",
+        )(result, new_state, new_conv)
         return result, new_state, new_conv.transpose(1, 0, 2)
     conv_part = sum(conv_state[:, i].astype(F32) * conv_taps[i] for i in range(3))
     branch_in, new_state, resid, n2 = pl.pallas_call(

time: 72.8 us -> 69.7 us (0.957)
  local copies, waits for them, and re-layouts: 5 us -> 0 us
  Pallas kernels: 66.9 us -> 68.9 us
    unnamed x3 -> x0, local copies, waits for them, and re-layouts: 5 us -> none
    pallas_call x0 -> x1, Pallas kernels: none -> 1.95 us  [per_device(): pl.pallas_call(emit_kernel, out_shape=tuple((jax.ShapeDtypeStruct(a.shape...]
where the time goes in v1:
time: 69.7 us; the launch traced here: 69.5 us
  Pallas kernels  68.9 us (99%)
    pallas_call x1, Pallas kernels, per_device(): pl.pallas_call(functools.partial(layer_kernel, peers), out_shape=(jax.Sha...  66.9 us
    pallas_call x1, Pallas kernels, per_device(): pl.pallas_call(emit_kernel, out_shape=tuple((jax.ShapeDtypeStruct(a.shape...  1.95 us

profile of v1, /device:TPU:0, one launch (start us, length us, event | category | flops | bytes accessed | tf_op | source)
XLA Modules:
  0.0 69.5 jit_solution(1665624344697670676)
XLA Ops:
  0.6 66.9 %layer.1 = (bf16[64,1024]{1,0:T(8,128)(2,1)}, f32[64,1024]{1,0:T(8,128)}, bf16[3,64,1024]{2,1,0:T(8,128)(2,1)}) custom-call(bf16[64,1024]{1,0:T(8,128)(2,1)} %stream_hbm.1, bf16[3,64,1024]{2,1,0:T(8,128)(2,1)} %bitcast.26, f32[64,1024]{1,0:T(8,128)} %state_hbm.1, f32[2,1,1024]{2,1,0:T(1,128)} %bitcast.27, bf16[2,1024,1024]{2,1,0:T(8,128)(2,1)} %bitcast.17, ...), custom_call_target="tpu_custom_call" | custom-call | tf_op jit(solution)/shard_map/layer/pallas_call | solution.py:837
  67.6 1.9 %emit.1 = (bf16[64,1024]{1,0:T(8,128)(2,1)}, f32[64,1024]{1,0:T(8,128)}, bf16[3,64,1024]{2,1,0:T(8,128)(2,1)}) custom-call(bf16[64,1024]{1,0:T(8,128)(2,1)} %get-tuple-element.9.a_in, f32[64,1024]{1,0:T(8,128)} %get-tuple-element.10.b_in, bf16[3,64,1024]{2,1,0:T(8,128)(2,1)} %get-tuple-element.11.c_in), custom_call_target="tpu_custom_call" | custom-call | tf_op jit(solution)/shard_map/emit/pallas_call | solution.py:868

commit v2 on v1

--- a/solution.py
+++ b/solution.py
@@ -175,9 +175,9 @@
     dg_hbm,
     du_hbm,
     dd_hbm,
-    result_ref,
-    new_state_ref,
-    new_conv_ref,
+    result_hbm,
+    new_state_hbm,
+    new_conv_hbm,
     stream_ref,
     conv_ref,
     state_ref,
@@ -199,35 +199,49 @@
     dg,
     du,
     dd,
+    result_ref,
+    new_state_ref,
+    new_conv_ref,
+    eg_peer,
+    eu_peer,
+    ed_peer,
     peer_ref,
     nrm_ref,
     mix_ref,
     res_ref,
+    dhid,
     inc,
-    hid,
-    dhid,
     snd,
-    zbuf,
     got_d,
+    got_dz,
     got_x,
     got_y,
+    zbuf,
     got_z,
+    fin_x,
+    fin_y,
+    fin_o,
     base_ref,
     wsend,
     wrecv,
     load_sem,
+    store_sem,
     m_send,
     m_recv,
+    mix_send,
+    mix_recv,
+    e_send,
+    e_recv,
     w_send,
     w_recv,
-    p_send,
-    p_recv,
-    h_send,
-    h_recv,
     link_send,
     link_recv,
     back_send,
     back_recv,
+    fin_send,
+    fin_recv,
+    dz_send,
+    dz_recv,
 ):
     e = lax.axis_index("ep")
     t = lax.axis_index("tp")
@@ -235,9 +249,11 @@
     depth = peers // 4
     z = e // 4
     q = e % 4
-    x_near = {"ep": 4 * z + flipped(q, 1)}
-    y_near = {"ep": 4 * z + flipped(q, 2)}
+    x_near = 4 * z + flipped(q, 1)
+    y_near = 4 * z + flipped(q, 2)
     rows, width = stream_ref.shape
+    half = rows // 2
+    mine = pl.ds(pl.multiple_of(half * t, half), half)
     pairs = (
         (stream_hbm, stream_ref),
         (gain_hbm, gain_ref),
@@ -269,15 +285,16 @@
 
     @pl.loop(1, peers)
     def _(offset):
-        pl.semaphore_signal(
-            barrier,
-            inc=1,
-            device_id={"ep": lax.rem(e + offset, peers)},
-            device_id_type=pl.DeviceIdType.MESH,
-        )
+        for core in range(2):
+            pl.semaphore_signal(
+                barrier,
+                inc=1,
+                device_id={"ep": lax.rem(e + offset, peers), "tp": core},
+                device_id_type=pl.DeviceIdType.MESH,
+            )
 
     loads[0].wait()
-    pl.semaphore_wait(barrier, peers)
+    pl.semaphore_wait(barrier, 2 * peers - 1)
     first = remote(stream_ref, peer_ref, m_send.at[0], m_recv.at[0], partner)
     first.start()
     own = stream_ref[...].astype(F32)
@@ -309,6 +326,11 @@
         load.wait()
     for i in (10, 11, 14, 15, 16, 17, 18, 19, 20):
         loads[i].start()
+    pushes = [
+        remote(a, b, e_send.at[i], e_recv.at[i], partner)
+        for i, (a, b) in enumerate(((eg_hbm, eg_peer), (eu_hbm, eu_peer), (ed_hbm, ed_peer)))
+    ]
+    pushes[0].start()
     block = rmap_ref.shape[1]
     chunk = 2 * block
     for c in range(width // chunk):
@@ -339,229 +361,429 @@
         new_state_ref[:, cols] = state
         gelu = 0.5 * gate * (1.0 + jnp.tanh(0.7978845608028654 * (gate + 0.044715 * gate**3)))
         mix_ref[0, :, cols] = (gelu * state).astype(BF16)
-    second = remote(mix_ref.at[0], mix_ref.at[1], m_send.at[1], m_recv.at[1], partner)
+    second = remote(mix_ref.at[0], mix_ref.at[1], mix_send.at[0], mix_recv.at[0], partner)
     second.start()
+    stores = [
+        pltpu.make_async_copy(new_state_ref, new_state_hbm, store_sem.at[0]),
+        pltpu.make_async_copy(new_conv_ref, new_conv_hbm, store_sem.at[1]),
+    ]
+    for store in stores:
+        store.start()
     loads[10].wait()
     mixed = dot(mix_ref[0], out_w[t])
     second.wait_recv()
     mixed = (mixed + dot(mix_ref[1], out_w[1 - t])).astype(BF16)
     resid = (own + mixed.astype(F32)).astype(BF16)
     res_ref[0] = resid
-    third = remote(res_ref.at[0], res_ref.at[1], m_send.at[2], m_recv.at[2], partner)
+    third = remote(res_ref.at[0], res_ref.at[1], m_send.at[1], m_recv.at[1], partner)
     third.start()
     resid = resid.astype(F32)
     sums = row_sums(resid)
     loads[11].wait()
     third.wait_recv()
     norm_pair(resid, sums, res_ref[1].astype(F32), gain2_ref, t, nrm_ref)
-    inc[0, 4 * z] = nrm_ref[0]
-    inc[1, 4 * z] = nrm_ref[1]
-
-    split = width // 2
+    inc[4 * z, t] = nrm_ref[0, mine, :]
+    inc[4 * z, 1 - t] = nrm_ref[1, mine, :]
+
+    turn = 1 + z // 2 * 2
+    mid = (z % 3 + 1) // 2
+    o_b = 2 + mid
+    o_c = 3 - mid
 
     def at(o):
-        return (z + depth - o) % depth
-
-    def z_copy(o):
-        there = {"ep": 4 * ((z + o) % depth) + q}
+        return (z + o * turn) % depth
+
+    def z_copy(o, h):
+        here = inc.at[4 * z, h]
+        there = {"ep": 4 * at(o) + q}
+        return remote(here, here, link_send.at[0, o, h], link_recv.at[0, z, h], there)
+
+    def z_relay(o, h):
+        j = at(o)
+        here = inc.at[4 * j, h]
+        there = {"ep": 4 * at(4 - o) + q}
+        return remote(here, here, dz_send.at[2, o - 1, h], link_recv.at[0, j, h], there)
+
+    def z_wait(o, h):
+        j = at(o)
+        here = inc.at[4 * j, h]
+        remote(here, here, link_send.at[0, j, h], link_recv.at[0, j, h], partner).wait_recv()
+
+    def side_copy(r, o, h):
+        j = at(o)
         return remote(
-            inc.at[0, 4 * z], inc.at[0, 4 * z], link_send.at[0, o], link_recv.at[0, z], there
-        )
-
-    def z_wait(o):
-        j = at(o)
-        mine = inc.at[0, 4 * j]
-        remote(mine, mine, link_send.at[0, o], link_recv.at[0, j], partner).wait_recv()
-
-    def side_copy(r, o):
+            inc.at[4 * j, h],
+            inc.at[4 * j + r, h],
+            link_send.at[r, j, h],
+            link_recv.at[r, j, h],
+            {"ep": x_near if r == 1 else y_near},
+        )
+
+    def d_copy(h, o):
         j = at(o)
         return remote(
-            inc.at[0, 4 * j],
-            inc.at[0, 4 * j + r],
-            link_send.at[r, j],
-            link_recv.at[r, j],
-            x_near if r == 1 else y_near,
-        )
-
-    def d_copy(r, o):
-        j = at(o)
-        cols = pl.ds((r - 1) * split, split)
+            inc.at[4 * j + 1 + h, h],
+            inc.at[4 * j + 3, h],
+            link_send.at[3, j, h],
+            link_recv.at[3, j, h],
+            {"ep": x_near if h else y_near},
+        )
+
+    def sides(o):
+        side_copy(1, o, 0).start()
+        side_copy(2, o, 1).start()
+        side_copy(1, o, 1).start()
+        side_copy(2, o, 0).start()
+
+    def along(o):
+        z_wait(o, 0)
+        if o != 2:
+
+            @pl.when(mid == 1)
+            def _():
+                z_relay(o, 0).start()
+
+        side_copy(1, o, 0).start()
+        z_wait(o, 1)
+        if o != 2:
+
+            @pl.when(mid == 1)
+            def _():
+                z_relay(o, 1).start()
+
+        side_copy(2, o, 1).start()
+        side_copy(1, o, 1).start()
+        side_copy(2, o, 0).start()
+
+    def dz_copy(o, h):
+        here = inc.at[4 * z + 3, h]
+        there = {"ep": 4 * at(o) + q}
+        return remote(here, here, dz_send.at[0, o, h], link_recv.at[3, z, h], there)
+
+    def dz_relay(o, h):
+        j = at(o)
+        here = inc.at[4 * j + 3, h]
+        there = {"ep": 4 * at(4 - o) + q}
+        return remote(here, here, dz_send.at[1, o, h], link_recv.at[3, j, h], there)
+
+    def dz():
+        for h in range(2):
+            d_copy(h, 0).wait_recv()
+            dz_copy(1, h).start()
+
+            @pl.when(mid == 1)
+            def _():
+                dz_copy(3, h).start()
+
+    def dzr():
+        @pl.when(mid == 1)
+        def _():
+            for h in range(2):
+                d_copy(h, 1).wait_recv()
+                dz_relay(1, h).start()
+
+    def near(o):
+        for h in range(2):
+            side_copy(1 + h, o, h).wait_recv()
+            d_copy(h, o).start()
+
+    def near_sides(o):
+        side_copy(1, o, 0).wait_recv()
+        side_copy(2, o, 1).wait_recv()
+
+    spread = lax.broadcasted_iota(jnp.int32, (half, lanes), 0) + half * t == (
+        lax.broadcasted_iota(jnp.int32, (half, lanes), 1)
+    )
+
+    def arrived_sides(o):
+        side_copy(1, o, 1).wait_recv()
+        side_copy(2, o, 0).wait_recv()
+
+    def arrived(o):
+        arrived_sides(o)
+        if not (isinstance(o, int) and o == 0):
+            for h in range(2):
+                d_copy(h, o).wait_recv()
+
+    def arr_end(o):
+        arrived_sides(o)
+
+        @pl.when(mid == 0)
+        def _():
+            for h in range(2):
+                d_copy(h, o).wait_recv()
+
+    def serve(o):
+        slot = 4 * at(o)
+        part = pl.ds(slot, 4)
+        cols = []
+        for r in range(4):
+            cols.append(jnp.sum(jnp.where(spread, wrecv[slot + r], 0.0), axis=1, keepdims=True))
+        scale = jnp.concatenate(cols, axis=0)
+        low = inc[part, 0].reshape(4 * half, width)
+        high = inc[part, 1].reshape(4 * half, width)
+        hidden = []
+        for gate_e, up_e in ((eg, eu), (eg_peer, eu_peer)):
+            gate = dot(low, gate_e[0]) + dot(high, gate_e[1])
+            up = dot(low, up_e[0]) + dot(high, up_e[1])
+            hidden.append((jax.nn.silu(gate) * up).astype(BF16))
+        for h, down in ((t, ed), (1 - t, ed_peer)):
+            served = (dot(hidden[0], down[t]) + dot(hidden[1], down[1 - t])) * scale
+            snd[part, h] = served.astype(BF16).reshape(4, half, width)
+
+    def d_back(h, o):
+        j = at(o)
         return remote(
-            inc.at[0, 4 * j + 3 - r, :, cols],
-            inc.at[0, 4 * j + 3, :, cols],
-            link_send.at[2 + r, j],
-            link_recv.at[2 + r, j],
-            x_near if r == 1 else y_near,
-        )
-
-    def p_copy(r, o):
-        slot = 4 * at(o) + r
-        return remote(inc.at[0, slot], inc.at[1, slot], p_send.at[slot], p_recv.at[slot], partner)
-
-    for o in range(1, depth):
-        z_copy(o).start()
-    side_copy(1, 0).start()
-    side_copy(2, 0).start()
+            snd.at[4 * j + 3, h],
+            got_d.at[j, h],
+            back_send.at[3, j, h],
+            back_recv.at[3, j, h],
+            {"ep": x_near if h else y_near},
+        )
+
+    def side_back(r, o, h):
+        j = at(o)
+        near_chip = x_near if r == 1 else y_near
+        if isinstance(o, int) and o == 0:
+            return remote(
+                snd.at[4 * j + r, h],
+                (fin_x if r == 1 else fin_y).at[mine],
+                back_send.at[r, j, h],
+                fin_recv.at[r, t],
+                {"ep": near_chip, "tp": h},
+            )
+        return remote(
+            snd.at[4 * j + r, h],
+            (got_x if r == 1 else got_y).at[j, h],
+            back_send.at[r, j, h],
+            back_recv.at[r, j, h],
+            {"ep": near_chip},
+        )
+
+    def dz_back(o, h):
+        j = at(o)
+        there = {"ep": 4 * j + q}
+        return remote(
+            snd.at[4 * j + 3, h], got_dz.at[z, h], dz_send.at[3, o, h], dz_recv.at[z, h], there
+        )
+
+    def dz_pass(h):
+        j = at(2)
+        there = {"ep": 4 * at(1) + q}
+        return remote(
+            snd.at[4 * j + 3, h], got_d.at[j, h], dz_send.at[3, 2, h], back_recv.at[3, j, h], there
+        )
+
+    def merge(slot, h, *parts):
+        total = snd[slot, h].astype(F32)
+        for part in parts:
+            total = total + part.astype(F32)
+        snd[slot, h] = total.astype(BF16)
+
+    def send_all(o):
+        for h in range(2):
+            side_back(1, o, h).start()
+            side_back(2, o, 1 - h).start()
+
+    def send_first(o):
+        d_back(0, o).start()
+        d_back(1, o).start()
+        side_back(1, o, 1).start()
+        side_back(2, o, 0).start()
+
+    def joined(o):
+        j = at(o)
+        for h in range(2):
+            d_back(h, o).wait_recv()
+            merge(4 * j + 1 + h, h, got_d[j, h])
+            side_back(1 + h, o, h).start()
+
+    def passed(o):
+        j = at(o)
+        for h in range(2):
+            d_back(h, o).wait_recv()
+            merge(4 * j + 3, h, got_d[j, h])
+            dz_back(o, h).start()
+
+    def dz_wait(o, h):
+        j = at(o)
+        here = got_dz.at[j, h]
+        remote(here, here, dz_send.at[3, o, h], dz_recv.at[j, h], partner).wait_recv()
+
+    def send_own():
+        @pl.when(mid == 1)
+        def _():
+            for h in range(2):
+                dz_wait(3, h)
+                merge(4 * z + 3, h, got_dz[at(3), h])
+
+        for h in range(2):
+            dz_wait(1, h)
+            merge(4 * z + 3, h, got_dz[at(1), h])
+            d_back(h, 0).start()
+
+    def bz_copy(o, h):
+        j = at(o)
+        return remote(
+            zbuf.at[j, h],
+            got_z.at[z, mine],
+            back_send.at[0, j, h],
+            back_recv.at[0, z, t],
+            {"ep": 4 * j + q, "tp": h},
+        )
+
+    def bz_wait(o, core):
+        j = at(o)
+        here = got_z.at[j, pl.ds(core * half, half)]
+        remote(here, here, back_send.at[0, j, 0], back_recv.at[0, j, core], partner).wait_recv()
+
+    def home(o):
+        j = at(o)
+        for h in range(2):
+            side_back(1, o, h).wait_recv()
+            side_back(2, o, h).wait_recv()
+            total = snd[4 * j, h].astype(F32) + got_x[j, h].astype(F32) + got_y[j, h].astype(F32)
+            zbuf[j, h] = total.astype(BF16)
+            bz_copy(o, h).start()
+
+    own_copy = remote(snd.at[4 * z, 1 - t], fin_o, fin_send.at[0], fin_recv.at[0, 0], partner)
+
+    for o in (1, 3):
+        for h in range(2):
+            z_copy(o, h).start()
+    sides(0)
+    pushes[1].start()
+    pushes[2].start()
 
     for load in loads[14:18]:
         load.wait()
     dense_gate = dot(nrm_ref[0], dg[t]) + dot(nrm_ref[1], dg[1 - t])
     dense_up = dot(nrm_ref[0], du[t]) + dot(nrm_ref[1], du[1 - t])
     dhid[0] = (jax.nn.silu(dense_gate) * dense_up).astype(BF16)
-    dense_copy = remote(dhid.at[0], dhid.at[1], m_send.at[3], m_recv.at[3], partner)
+    dense_copy = remote(dhid.at[0], dhid.at[1], m_send.at[2], m_recv.at[2], partner)
     dense_copy.start()
-
-    def along(o):
-        z_wait(o)
-        side_copy(1, o).start()
-        side_copy(2, o).start()
-        p_copy(0, o).start()
-
-    def near(o):
-        side_copy(1, o).wait_recv()
-        d_copy(2, o).start()
-        p_copy(1, o).start()
-        side_copy(2, o).wait_recv()
-        d_copy(1, o).start()
-        p_copy(2, o).start()
-
-    def h_copy(o):
-        part = pl.ds(4 * at(o), 4)
-        return remote(hid.at[0, part], hid.at[1, part], h_send.at[o], h_recv.at[o], partner)
-
-    def upward(o):
-        for r in range(4):
-            if r or o:
-                p_copy(r, o).wait_recv()
-        part = pl.ds(4 * at(o), 4)
-        mine = inc[0, part].reshape(4 * rows, width)
-        peer = inc[1, part].reshape(4 * rows, width)
-        gate = dot(mine, eg[t]) + dot(peer, eg[1 - t])
-        up = dot(mine, eu[t]) + dot(peer, eu[1 - t])
-        hid[0, part] = (jax.nn.silu(gate) * up).astype(BF16).reshape(4, rows, -1)
-        h_copy(o).start()
-
-    spread = lax.broadcasted_iota(jnp.int32, (rows, lanes), 0) == lax.broadcasted_iota(
-        jnp.int32, (rows, lanes), 1
-    )
-
-    def downward(o):
-        base_slot = 4 * at(o)
-        part = pl.ds(base_slot, 4)
-        cols = []
-        for r in range(4):
-            row = wrecv[base_slot + r]
-            cols.append(jnp.sum(jnp.where(spread, row, 0.0), axis=1, keepdims=True))
-        h_copy(o).wait_recv()
-        mine = hid[0, part].reshape(4 * rows, -1)
-        peer = hid[1, part].reshape(4 * rows, -1)
-        served = dot(mine, ed[t]) + dot(peer, ed[1 - t])
-        served = served * jnp.concatenate(cols, axis=0)
-        snd[part] = served.astype(BF16).reshape(4, rows, width)
-        bd_copy(1, o).start()
-        bd_copy(2, o).start()
-
-    def bd_copy(r, o):
-        j = at(o)
-        cols = pl.ds((r - 1) * split, split)
-        return remote(
-            snd.at[4 * j + 3, :, cols],
-            got_d.at[j, :, cols],
-            back_send.at[2 + r, j],
-            back_recv.at[2 + r, j],
-            x_near if r == 1 else y_near,
-        )
-
-    def side_back(r, o):
-        j = at(o)
-        return remote(
-            snd.at[4 * j + r],
-            (got_x if r == 1 else got_y).at[j],
-            back_send.at[r, j],
-            back_recv.at[r, j],
-            x_near if r == 1 else y_near,
-        )
-
-    def bz_copy(o):
-        j = at(o)
-        there = {"ep": 4 * j + q}
-        return remote(zbuf.at[j], got_z.at[z], back_send.at[0, j], back_recv.at[0, z], there)
-
-    def bz_wait(o):
-        j = at(o)
-        remote(zbuf.at[j], got_z.at[j], back_send.at[0, j], back_recv.at[0, j], partner).wait_recv()
-
-    def joined(o):
-        j = at(o)
-        for r in (1, 2):
-            bd_copy(r, o).wait_recv()
-            cols = pl.ds((r - 1) * split, split)
-            slot = 4 * j + 3 - r
-            both = snd[slot, :, cols].astype(F32) + got_d[j, :, cols].astype(F32)
-            snd[slot, :, cols] = both.astype(BF16)
-            side_back(3 - r, o).start()
-
-    def summed(o):
-        j = at(o)
-        side_back(1, o).wait_recv()
-        side_back(2, o).wait_recv()
-        total = snd[4 * j].astype(F32) + got_x[j].astype(F32) + got_y[j].astype(F32)
-        if o:
-            zbuf[j] = total.astype(BF16)
-            bz_copy(o).start()
-        return total
-
+    near(0)
     along(1)
-    near(0)
     for r, o in places:
-        slot = 4 * at(o) + r
+        slot = 4 * ((z + o) % depth) + r
         remote(wsend.at[0], wrecv.at[slot], w_send.at[0], w_recv.at[slot], partner).wait_recv()
-    mine = jnp.sum(jnp.where(ids == e, weights, 0.0), axis=0, keepdims=True)
-    wrecv[4 * z] = jnp.concatenate([mine, jnp.zeros((1, lanes - rows), F32)], axis=1)
+    row = jnp.sum(jnp.where(ids == e, weights, 0.0), axis=0, keepdims=True)
+    wrecv[4 * z] = jnp.concatenate([row, jnp.zeros((1, lanes - rows), F32)], axis=1)
     dense = dot(dhid[0], dd[t])
     dense_copy.wait_recv()
     dense = (dense + dot(dhid[1], dd[1 - t])).astype(BF16)
     base_ref[...] = resid + scale_ref[...] * dense.astype(F32)
     for load in loads[18:]:
         load.wait()
-
-    for step in range(1, depth + 3):
-        if step + 1 < depth:
-            along(step + 1)
-        if step < depth:
-            near(step)
-        if step <= depth:
-            d_copy(1, step - 1).wait_recv()
-            d_copy(2, step - 1).wait_recv()
-            p_copy(3, step - 1).start()
-        if 2 <= step <= depth + 1:
-            joined(step - 2)
-        if step <= depth:
-            upward(step - 1)
-            downward(step - 1)
-        if 3 <= step:
-            part_sum = summed(step - 3)
-            if step == 3:
-                base_ref[...] += part_sum
+    for push in pushes:
+        push.wait_recv()
+    along(3)
+    dz()
+    along(2)
+    arrived(0)
+    serve(0)
+    own_copy.start()
+    near(o_c)
+    dzr()
+    near_sides(1)
+    arr_end(1)
+    serve(1)
+    send_all(1)
+
+    @pl.when(mid == 0)
+    def _():
+        dz_back(1, 0).start()
+        dz_back(1, 1).start()
+
+    near_sides(o_b)
+    arrived(o_b)
+    serve(o_b)
+
+    @pl.when(mid == 0)
+    def _():
+        dz_pass(0).start()
+        dz_pass(1).start()
+
+
+    @pl.when(mid == 1)
+    def _():
+        dz_back(3, 0).start()
+        dz_back(3, 1).start()
+
+    send_all(o_b)
+    arrived(o_c)
+    serve(o_c)
+    send_first(o_c)
+    home(1)
+
+    @pl.when(mid == 1)
+    def _():
+        passed(1)
+
+    joined(o_c)
+    side_back(1, 0, 1).start()
+    side_back(2, 0, 0).start()
+    home(o_b)
+    home(o_c)
+    send_own()
+    joined(0)
+    other = pl.ds(pl.multiple_of(half - half * t, half), half)
+    base_ref[mine, :] += snd[4 * z, t].astype(F32)
+    own_copy.wait_recv()
+    base_ref[other, :] += fin_o[...].astype(F32)
     total = base_ref[...]
     for o in range(1, depth):
-        bz_wait(o)
+        for core in range(2):
+            bz_wait(o, core)
         total = total + got_z[at(o)].astype(F32)
+    for r, fin in ((1, fin_x), (2, fin_y)):
+        for core in range(2):
+            here = fin.at[pl.ds(core * half, half)]
+            remote(here, here, fin_send.at[1], fin_recv.at[r, core], partner).wait_recv()
+        total = total + fin[...].astype(F32)
     result_ref[...] = total.astype(BF16)
-
-    for copy in (first, second, third, dense_copy):
+    stores.append(pltpu.make_async_copy(result_ref, result_hbm, store_sem.at[2]))
+    stores[-1].start()
+    for copy in (first, third, dense_copy, own_copy, second, *pushes):
         copy.wait_send()
     for r, o in places:
         weighing(r, o).wait_send()
-        p_copy(r, o).wait_send()
     for o in range(depth):
-        h_copy(o).wait_send()
-        if o:
-            z_copy(o).wait_send()
-            bz_copy(o).wait_send()
-        for r in (1, 2):
-            for copy in (side_copy, d_copy, side_back, bd_copy):
-                copy(r, o).wait_send()
+        for h in range(2):
+            if o:
+                bz_copy(o, h).wait_send()
+            if o in (1, 3):
+                z_copy(o, h).wait_send()
+            for r in (1, 2):
+                side_copy(r, o, h).wait_send()
+                side_back(r, o, h).wait_send()
+        if o == 0:
+            for h in range(2):
+                d_copy(h, o).wait_send()
+                d_back(h, o).wait_send()
+
+    @pl.when(mid == 1)
+    def _():
+        for h in range(2):
+            z_relay(1, h).wait_send()
+            z_relay(3, h).wait_send()
+            dz_relay(1, h).wait_send()
+            dz_copy(3, h).wait_send()
+            dz_back(3, h).wait_send()
+
+    @pl.when(mid == 0)
+    def _():
+        for h in range(2):
+            dz_pass(h).wait_send()
+
+    for h in range(2):
+        d_copy(h, o_c).wait_send()
+        d_back(h, o_c).wait_send()
+        dz_copy(1, h).wait_send()
+        dz_back(1, h).wait_send()
+
+    for store in stores:
+        store.wait()
 
 
 def expert_kernel(
@@ -806,7 +1028,7 @@
     top = route_ids.shape[1]
     peers = lax.axis_size("ep")
     cap = max(2, min(rows, 3 * rows * top // peers))
-    if cap == rows and peers % 8 == 0:
+    if cap == rows and peers // 4 == 4:
         operands = (
             stream,
             conv_state.transpose(1, 0, 2),
@@ -831,35 +1053,37 @@
             halves(dense_down),
         )
         depth = peers // 4
-        hidden = expert_gate.shape[2]
+        half = rows // 2
         lanes = -(-rows // 128) * 128
-        column = pltpu.VMEM((depth, rows, width), BF16)
+        outs = (
+            jax.ShapeDtypeStruct((rows, width), BF16),
+            jax.ShapeDtypeStruct((rows, width), F32),
+            jax.ShapeDtypeStruct((3, rows, width), BF16),
+        )
+        column = pltpu.VMEM((depth, 2, half, width), BF16)
+        whole = pltpu.VMEM((rows, width), BF16)
         result, new_state, new_conv = pl.pallas_call(
             functools.partial(layer_kernel, peers),
-            out_shape=(
-                jax.ShapeDtypeStruct((rows, width), BF16),
-                jax.ShapeDtypeStruct((rows, width), F32),
-                jax.ShapeDtypeStruct((3, rows, width), BF16),
-            ),
-            in_specs=[HBM] * len(operands),
-            out_specs=[VMEM] * 3,
-            scratch_shapes=[pltpu.VMEM(a.shape, a.dtype) for a in operands]
-            + [pltpu.VMEM((rows, width), BF16)]
+            out_shape=outs,
+            in_specs=[ANY] * len(operands),
+            out_specs=[ANY] * 3,
+            scratch_shapes=[pltpu.VMEM(a.shape, a.dtype) for a in operands + outs + operands[15:18]]
+            + [whole]
             + [pltpu.VMEM((2, rows, width), BF16)] * 3
-            + [
-                pltpu.VMEM((2, peers, rows, width), BF16),
-                pltpu.VMEM((2, peers, rows, hidden), BF16),
-                pltpu.VMEM((2, rows, dense_gate.shape[1]), BF16),
-                pltpu.VMEM((peers, rows, width), BF16),
-            ]
+            + [pltpu.VMEM((2, rows, dense_gate.shape[1]), BF16)]
+            + [pltpu.VMEM((peers, 2, half, width), BF16)] * 2
             + [column] * 5
-            + [pltpu.VMEM((rows, width), F32)]
+            + [pltpu.VMEM((depth, rows, width), BF16)]
+            + [whole] * 2
+            + [pltpu.VMEM((half, width), BF16), pltpu.VMEM((rows, width), F32)]
             + [pltpu.VMEM((peers, 1, lanes), F32)] * 2
-            + [dma((len(operands),))]
-            + [dma((4,))] * 2
-            + [dma((peers,))] * 4
-            + [dma((depth,))] * 2
-            + [dma((5, depth))] * 4,
+            + [dma((len(operands),)), dma((3,))]
+            + [dma((3,))] * 2
+            + [dma((1,))] * 2
+            + [dma((3,))] * 2
+            + [dma((peers,))] * 2
+            + [dma((4, depth, 2))] * 4
+            + [dma((2,)), dma((3, 2)), dma((4, depth, 2)), dma((depth, 2))],
             compiler_params=pltpu.CompilerParams(
                 collective_id=2, has_side_effects=True, vmem_limit_bytes=63 * 1024 * 1024
             ),

time: 69.7 us -> 57.4 us (0.82)
  the two profiles are of different devices: /device:TPU:0 before, /device:TPU:11 now
where the time goes in v2:
time: 57.4 us; the launch traced here: 57.3 us
  Pallas kernels  56.6 us (99%)
  between operations  0.65 us (1%)
    pallas_call x1, Pallas kernels, per_device(): pl.pallas_call(functools.partial(layer_kernel, peers), out_shape=outs, in...  54.7 us
    pallas_call x1, Pallas kernels, per_device(): pl.pallas_call(emit_kernel, out_shape=tuple((jax.ShapeDtypeStruct(a.shape...  1.95 us

profile of v2, /device:TPU:11, one launch (start us, length us, event | category | flops | bytes accessed | tf_op | source)
XLA Modules:
  0.0 57.3 jit_solution(8168089157023212642)
XLA Ops:
  0.6 54.7 %layer.1 = (bf16[64,1024]{1,0:T(8,128)(2,1)}, f32[64,1024]{1,0:T(8,128)}, bf16[3,64,1024]{2,1,0:T(8,128)(2,1)}) custom-call(bf16[64,1024]{1,0:T(8,128)(2,1)} %stream_hbm.1, bf16[3,64,1024]{2,1,0:T(8,128)(2,1)} %bitcast.26, f32[64,1024]{1,0:T(8,128)} %state_hbm.1, f32[2,1,1024]{2,1,0:T(1,128)} %bitcast.27, bf16[2,1024,1024]{2,1,0:T(8,128)(2,1)} %bitcast.17, ...), custom_call_target="tpu_custom_call" | custom-call | tf_op jit(solution)/shard_map/layer/pallas_call | solution.py:1065
  55.3 1.9 %emit.1 = (bf16[64,1024]{1,0:T(8,128)(2,1)}, f32[64,1024]{1,0:T(8,128)}, bf16[3,64,1024]{2,1,0:T(8,128)(2,1)}) custom-call(bf16[64,1024]{1,0:T(8,128)(2,1)} %get-tuple-element.9.a_in, f32[64,1024]{1,0:T(8,128)} %get-tuple-element.10.b_in, bf16[3,64,1024]{2,1,0:T(8,128)(2,1)} %get-tuple-element.11.c_in), custom_call_target="tpu_custom_call" | custom-call | tf_op jit(solution)/shard_map/emit/pallas_call | solution.py:1092

commit v3 on v2

--- a/solution.py
+++ b/solution.py
@@ -370,9 +370,9 @@
     for store in stores:
         store.start()
     loads[10].wait()
-    mixed = dot(mix_ref[0], out_w[t])
+    base_ref[...] = dot(mix_ref[0], out_w[t])
     second.wait_recv()
-    mixed = (mixed + dot(mix_ref[1], out_w[1 - t])).astype(BF16)
+    mixed = (base_ref[...] + dot(mix_ref[1], out_w[1 - t])).astype(BF16)
     resid = (own + mixed.astype(F32)).astype(BF16)
     res_ref[0] = resid
     third = remote(res_ref.at[0], res_ref.at[1], m_send.at[1], m_recv.at[1], partner)
@@ -435,25 +435,28 @@
         side_copy(1, o, 1).start()
         side_copy(2, o, 0).start()
 
+    def z_in(o, h):
+        z_wait(o, h)
+        z_relay(o, h).start()
+
     def along(o):
         z_wait(o, 0)
-        if o != 2:
-
-            @pl.when(mid == 1)
-            def _():
-                z_relay(o, 0).start()
-
         side_copy(1, o, 0).start()
         z_wait(o, 1)
-        if o != 2:
-
-            @pl.when(mid == 1)
-            def _():
-                z_relay(o, 1).start()
-
         side_copy(2, o, 1).start()
         side_copy(1, o, 1).start()
         side_copy(2, o, 0).start()
+
+    def along_both():
+        z_in(1, 0)
+        side_copy(1, 1, 0).start()
+        z_in(3, 0)
+        side_copy(1, 3, 0).start()
+        for o in (1, 3):
+            z_in(o, 1)
+            side_copy(2, o, 1).start()
+            side_copy(1, o, 1).start()
+            side_copy(2, o, 0).start()
 
     def dz_copy(o, h):
         here = inc.at[4 * z + 3, h]
@@ -567,13 +570,6 @@
             snd.at[4 * j + 3, h], got_dz.at[z, h], dz_send.at[3, o, h], dz_recv.at[z, h], there
         )
 
-    def dz_pass(h):
-        j = at(2)
-        there = {"ep": 4 * at(1) + q}
-        return remote(
-            snd.at[4 * j + 3, h], got_d.at[j, h], dz_send.at[3, 2, h], back_recv.at[3, j, h], there
-        )
-
     def merge(slot, h, *parts):
         total = snd[slot, h].astype(F32)
         for part in parts:
@@ -598,13 +594,6 @@
             merge(4 * j + 1 + h, h, got_d[j, h])
             side_back(1 + h, o, h).start()
 
-    def passed(o):
-        j = at(o)
-        for h in range(2):
-            d_back(h, o).wait_recv()
-            merge(4 * j + 3, h, got_d[j, h])
-            dz_back(o, h).start()
-
     def dz_wait(o, h):
         j = at(o)
         here = got_dz.at[j, h]
@@ -615,7 +604,8 @@
         def _():
             for h in range(2):
                 dz_wait(3, h)
-                merge(4 * z + 3, h, got_dz[at(3), h])
+                dz_wait(2, h)
+                merge(4 * z + 3, h, got_dz[at(3), h], got_dz[at(2), h])
 
         for h in range(2):
             dz_wait(1, h)
@@ -663,7 +653,15 @@
     dense_copy = remote(dhid.at[0], dhid.at[1], m_send.at[2], m_recv.at[2], partner)
     dense_copy.start()
     near(0)
-    along(1)
+
+    @pl.when(mid == 1)
+    def _():
+        along_both()
+
+    @pl.when(mid == 0)
+    def _():
+        along(1)
+
     for r, o in places:
         slot = 4 * ((z + o) % depth) + r
         remote(wsend.at[0], wrecv.at[slot], w_send.at[0], w_recv.at[slot], partner).wait_recv()
@@ -677,62 +675,96 @@
         load.wait()
     for push in pushes:
         push.wait_recv()
-    along(3)
+
+    @pl.when(mid == 0)
+    def _():
+        along(3)
+
     dz()
     along(2)
     arrived(0)
     serve(0)
     own_copy.start()
+    dzr()
     near(o_c)
-    dzr()
     near_sides(1)
     arr_end(1)
     serve(1)
-    send_all(1)
-
-    @pl.when(mid == 0)
+
+    @pl.when(mid == 1)
     def _():
         dz_back(1, 0).start()
         dz_back(1, 1).start()
 
-    near_sides(o_b)
-    arrived(o_b)
-    serve(o_b)
 
     @pl.when(mid == 0)
     def _():
-        dz_pass(0).start()
-        dz_pass(1).start()
-
+        dz_back(1, 0).start()
+        dz_back(1, 1).start()
+
+    send_all(1)
+
+    @pl.when(mid == 1)
+    def _():
+        near_sides(3)
+
+    arrived(3)
+    serve(3)
 
     @pl.when(mid == 1)
     def _():
         dz_back(3, 0).start()
         dz_back(3, 1).start()
-
-    send_all(o_b)
-    arrived(o_c)
-    serve(o_c)
-    send_first(o_c)
+        side_back(1, 3, 0).start()
+        side_back(2, 3, 1).start()
+
+
+    @pl.when(mid == 0)
+    def _():
+        send_first(3)
+
+
+    @pl.when(mid == 0)
+    def _():
+        near_sides(2)
+
+    arrived(2)
+    serve(2)
+
+    @pl.when(mid == 0)
+    def _():
+        dz_back(2, 0).start()
+        dz_back(2, 1).start()
+        side_back(1, 2, 0).start()
+        side_back(2, 2, 1).start()
+
+
+    @pl.when(mid == 1)
+    def _():
+        send_first(2)
+        side_back(1, 3, 1).start()
+        side_back(2, 3, 0).start()
+
     home(1)
-
-    @pl.when(mid == 1)
-    def _():
-        passed(1)
-
     joined(o_c)
+
+    @pl.when(mid == 0)
+    def _():
+        side_back(1, 2, 1).start()
+        side_back(2, 2, 0).start()
+
     side_back(1, 0, 1).start()
     side_back(2, 0, 0).start()
+    send_own()
+    home(o_c)
     home(o_b)
-    home(o_c)
-    send_own()
     joined(0)
     other = pl.ds(pl.multiple_of(half - half * t, half), half)
     base_ref[mine, :] += snd[4 * z, t].astype(F32)
     own_copy.wait_recv()
     base_ref[other, :] += fin_o[...].astype(F32)
     total = base_ref[...]
-    for o in range(1, depth):
+    for o in (1, 3, 2):
         for core in range(2):
             bz_wait(o, core)
         total = total + got_z[at(o)].astype(F32)
@@ -774,7 +806,7 @@
     @pl.when(mid == 0)
     def _():
         for h in range(2):
-            dz_pass(h).wait_send()
+            dz_back(2, h).wait_send()
 
     for h in range(2):
         d_copy(h, o_c).wait_send()

time: 57.4 us -> 54 us (0.941)
  the two profiles are of different devices: /device:TPU:11 before, /device:TPU:0 now
where the time goes in v3:
time: 54 us; the launch traced here: 53.2 us
  Pallas kernels  52.6 us (97%)
  between operations  0.65 us (1%)
    pallas_call x1, Pallas kernels, per_device(): pl.pallas_call(functools.partial(layer_kernel, peers), out_shape=outs, in...  50.6 us
    pallas_call x1, Pallas kernels, per_device(): pl.pallas_call(emit_kernel, out_shape=tuple((jax.ShapeDtypeStruct(a.shape...  1.95 us

profile of v3, /device:TPU:0, one launch (start us, length us, event | category | flops | bytes accessed | tf_op | source)
XLA Modules:
  0.0 53.2 jit_solution(11118090518183696100)
XLA Ops:
  0.6 50.6 %layer.1 = (bf16[64,1024]{1,0:T(8,128)(2,1)}, f32[64,1024]{1,0:T(8,128)}, bf16[3,64,1024]{2,1,0:T(8,128)(2,1)}) custom-call(bf16[64,1024]{1,0:T(8,128)(2,1)} %stream_hbm.1, bf16[3,64,1024]{2,1,0:T(8,128)(2,1)} %bitcast.26, f32[64,1024]{1,0:T(8,128)} %state_hbm.1, f32[2,1,1024]{2,1,0:T(1,128)} %bitcast.27, bf16[2,1024,1024]{2,1,0:T(8,128)(2,1)} %bitcast.17, ...), custom_call_target="tpu_custom_call" | custom-call | tf_op jit(solution)/shard_map/layer/pallas_call | solution.py:1097
  51.3 1.9 %emit.1 = (bf16[64,1024]{1,0:T(8,128)(2,1)}, f32[64,1024]{1,0:T(8,128)}, bf16[3,64,1024]{2,1,0:T(8,128)(2,1)}) custom-call(bf16[64,1024]{1,0:T(8,128)(2,1)} %get-tuple-element.9.a_in, f32[64,1024]{1,0:T(8,128)} %get-tuple-element.10.b_in, bf16[3,64,1024]{2,1,0:T(8,128)(2,1)} %get-tuple-element.11.c_in), custom_call_target="tpu_custom_call" | custom-call | tf_op jit(solution)/shard_map/emit/pallas_call | solution.py:1124

commit v4 on v3

--- a/solution.py
+++ b/solution.py
@@ -242,6 +242,8 @@
     fin_recv,
     dz_send,
     dz_recv,
+    res_send,
+    res_recv,
 ):
     e = lax.axis_index("ep")
     t = lax.axis_index("tp")
@@ -375,13 +377,25 @@
     mixed = (base_ref[...] + dot(mix_ref[1], out_w[1 - t])).astype(BF16)
     resid = (own + mixed.astype(F32)).astype(BF16)
     res_ref[0] = resid
-    third = remote(res_ref.at[0], res_ref.at[1], m_send.at[1], m_recv.at[1], partner)
-    third.start()
+    other = pl.ds(pl.multiple_of(half - half * t, half), half)
+
+    def res_copy(part, i):
+        here, there = res_ref.at[0, part], res_ref.at[1, part]
+        return remote(here, there, res_send.at[i], res_recv.at[i], partner)
+
+    res_copy(other, 0).start()
+    res_copy(mine, 1).start()
     resid = resid.astype(F32)
-    sums = row_sums(resid)
     loads[11].wait()
-    third.wait_recv()
-    norm_pair(resid, sums, res_ref[1].astype(F32), gain2_ref, t, nrm_ref)
+    base_ref[...] = resid
+    res_copy(mine, 0).wait_recv()
+
+    def norm_part(part):
+        rows_f = base_ref[part, :]
+        peer_f = res_ref[1, part, :].astype(F32)
+        norm_pair(rows_f, row_sums(rows_f), peer_f, gain2_ref, t, nrm_ref.at[:, part, :])
+
+    norm_part(mine)
     inc[4 * z, t] = nrm_ref[0, mine, :]
     inc[4 * z, 1 - t] = nrm_ref[1, mine, :]
 
@@ -482,8 +496,9 @@
         @pl.when(mid == 1)
         def _():
             for h in range(2):
-                d_copy(h, 1).wait_recv()
-                dz_relay(1, h).start()
+                for o in (3, 1):
+                    d_copy(h, o).wait_recv()
+                    dz_relay(o, h).start()
 
     def near(o):
         for h in range(2):
@@ -647,6 +662,8 @@
 
     for load in loads[14:18]:
         load.wait()
+    res_copy(other, 1).wait_recv()
+    norm_part(other)
     dense_gate = dot(nrm_ref[0], dg[t]) + dot(nrm_ref[1], dg[1 - t])
     dense_up = dot(nrm_ref[0], du[t]) + dot(nrm_ref[1], du[1 - t])
     dhid[0] = (jax.nn.silu(dense_gate) * dense_up).astype(BF16)
@@ -686,80 +703,96 @@
     serve(0)
     own_copy.start()
     dzr()
-    near(o_c)
+
+    @pl.when(mid == 0)
+    def _():
+        near(3)
+
+
+    @pl.when(mid == 1)
+    def _():
+        near_sides(2)
+
     near_sides(1)
     arr_end(1)
     serve(1)
+    dz_back(1, 0).start()
+    dz_back(1, 1).start()
+    side_back(1, 1, 0).start()
+    side_back(2, 1, 1).start()
 
     @pl.when(mid == 1)
     def _():
-        dz_back(1, 0).start()
-        dz_back(1, 1).start()
+        near_sides(3)
+        arrived_sides(3)
 
 
     @pl.when(mid == 0)
     def _():
-        dz_back(1, 0).start()
-        dz_back(1, 1).start()
-
-    send_all(1)
-
-    @pl.when(mid == 1)
-    def _():
-        near_sides(3)
-
-    arrived(3)
+        arrived(3)
+
     serve(3)
 
     @pl.when(mid == 1)
     def _():
         dz_back(3, 0).start()
         dz_back(3, 1).start()
+
+
+    @pl.when(mid == 0)
+    def _():
+        send_first(3)
+
+    side_back(1, 1, 1).start()
+    side_back(2, 1, 0).start()
+
+    @pl.when(mid == 0)
+    def _():
+        near_sides(2)
+
+    arrived(2)
+    serve(2)
+
+    @pl.when(mid == 0)
+    def _():
+        dz_back(2, 0).start()
+        dz_back(2, 1).start()
+
+
+    @pl.when(mid == 1)
+    def _():
+        send_first(2)
         side_back(1, 3, 0).start()
         side_back(2, 3, 1).start()
 
 
+    @pl.when(mid == 1)
+    def _():
+        home(1)
+
+    joined(o_c)
+
     @pl.when(mid == 0)
     def _():
-        send_first(3)
-
-
-    @pl.when(mid == 0)
-    def _():
-        near_sides(2)
-
-    arrived(2)
-    serve(2)
-
-    @pl.when(mid == 0)
-    def _():
-        dz_back(2, 0).start()
-        dz_back(2, 1).start()
-        side_back(1, 2, 0).start()
-        side_back(2, 2, 1).start()
+        send_all(2)
 
 
     @pl.when(mid == 1)
     def _():
-        send_first(2)
         side_back(1, 3, 1).start()
         side_back(2, 3, 0).start()
 
-    home(1)
-    joined(o_c)
-
-    @pl.when(mid == 0)
-    def _():
-        side_back(1, 2, 1).start()
-        side_back(2, 2, 0).start()
-
     side_back(1, 0, 1).start()
     side_back(2, 0, 0).start()
+
+    @pl.when(mid == 0)
+    def _():
+        home(1)
+
     send_own()
     home(o_c)
     home(o_b)
     joined(0)
-    other = pl.ds(pl.multiple_of(half - half * t, half), half)
     base_ref[mine, :] += snd[4 * z, t].astype(F32)
     own_copy.wait_recv()
     base_ref[other, :] += fin_o[...].astype(F32)
@@ -776,7 +809,9 @@
     result_ref[...] = total.astype(BF16)
     stores.append(pltpu.make_async_copy(result_ref, result_hbm, store_sem.at[2]))
     stores[-1].start()
-    for copy in (first, third, dense_copy, own_copy, second, *pushes):
+    res_copy(other, 0).wait_send()
+    res_copy(mine, 1).wait_send()
+    for copy in (first, dense_copy, own_copy, second, *pushes):
         copy.wait_send()
     for r, o in places:
         weighing(r, o).wait_send()
@@ -800,6 +835,7 @@
             z_relay(1, h).wait_send()
             z_relay(3, h).wait_send()
             dz_relay(1, h).wait_send()
+            dz_relay(3, h).wait_send()
             dz_copy(3, h).wait_send()
             dz_back(3, h).wait_send()
 
@@ -807,9 +843,9 @@
     def _():
         for h in range(2):
             dz_back(2, h).wait_send()
+            d_copy(h, 3).wait_send()
 
     for h in range(2):
-        d_copy(h, o_c).wait_send()
         d_back(h, o_c).wait_send()
         dz_copy(1, h).wait_send()
         dz_back(1, h).wait_send()
@@ -1115,7 +1151,8 @@
             + [dma((3,))] * 2
             + [dma((peers,))] * 2
             + [dma((4, depth, 2))] * 4
-            + [dma((2,)), dma((3, 2)), dma((4, depth, 2)), dma((depth, 2))],
+            + [dma((2,)), dma((3, 2)), dma((4, depth, 2)), dma((depth, 2))]
+            + [dma((2,))] * 2,
             compiler_params=pltpu.CompilerParams(
                 collective_id=2, has_side_effects=True, vmem_limit_bytes=63 * 1024 * 1024
             ),

time: 54 us -> 53.2 us (0.985)
  no operation moved by 1% of the time
where the time goes in v4:
time: 53.2 us; the launch traced here: 52.9 us
  Pallas kernels  52.3 us (98%)
  between operations  0.65 us (1%)
    pallas_call x1, Pallas kernels, per_device(): pl.pallas_call(functools.partial(layer_kernel, peers), out_shape=outs, in...  50.3 us
    pallas_call x1, Pallas kernels, per_device(): pl.pallas_call(emit_kernel, out_shape=tuple((jax.ShapeDtypeStruct(a.shape...  1.95 us

profile of v4, /device:TPU:0, one launch (start us, length us, event | category | flops | bytes accessed | tf_op | source)
XLA Modules:
  0.0 52.9 jit_solution(5712977040417934432)
XLA Ops:
  0.6 50.3 %layer.1 = (bf16[64,1024]{1,0:T(8,128)(2,1)}, f32[64,1024]{1,0:T(8,128)}, bf16[3,64,1024]{2,1,0:T(8,128)(2,1)}) custom-call(bf16[64,1024]{1,0:T(8,128)(2,1)} %stream_hbm.1, bf16[3,64,1024]{2,1,0:T(8,128)(2,1)} %bitcast.26, f32[64,1024]{1,0:T(8,128)} %state_hbm.1, f32[2,1,1024]{2,1,0:T(1,128)} %bitcast.27, bf16[2,1024,1024]{2,1,0:T(8,128)(2,1)} %bitcast.17, ...), custom_call_target="tpu_custom_call" | custom-call | tf_op jit(solution)/shard_map/layer/pallas_call | solution.py:1133
  51.0 1.9 %emit.1 = (bf16[64,1024]{1,0:T(8,128)(2,1)}, f32[64,1024]{1,0:T(8,128)}, bf16[3,64,1024]{2,1,0:T(8,128)(2,1)}) custom-call(bf16[64,1024]{1,0:T(8,128)(2,1)} %get-tuple-element.9.a_in, f32[64,1024]{1,0:T(8,128)} %get-tuple-element.10.b_in, bf16[3,64,1024]{2,1,0:T(8,128)(2,1)} %get-tuple-element.11.c_in), custom_call_target="tpu_custom_call" | custom-call | tf_op jit(solution)/shard_map/emit/pallas_call | solution.py:1161
